TPU v7x, 32 devices: a whole 2x2x4 slice. The times are simulated.
32 devices in a mesh: kv: 4 (over y, x), tp: 8 (over z, core).
Axes of the slice: x: 2, y: 2, z: 4, core: 2. Of those that a mesh axis runs over, the one named last changes fastest.
Arguments:
- hidden_in: bfloat16 [16, 4096], P('kv', 'tp'), may hold values from -12 to 12
- mixer_gain: float32 [4096], P('tp'), may hold values from 0.1 to 1.9
- query_weight: bfloat16 [4096, 4096], P('tp', 'kv'), may hold values from -0.09375 to 0.09375
- key_weight: bfloat16 [4096, 4096], P('tp', 'kv'), may hold values from -0.09375 to 0.09375
- value_weight: bfloat16 [4096, 8192], P('tp', 'kv'), may hold values from -0.09375 to 0.09375
- gate_weight: bfloat16 [4096, 8192], P('tp', 'kv'), may hold values from -0.09375 to 0.09375
- decay_rate: float32 [16], P('kv'), may hold values from 0.0005 to 0.15
- prior_state: float32 [16, 16, 256, 512], P('tp', 'kv'), may hold values from -2.5 to 2.5
- key_block: bfloat16 [16, 16, 128, 256], P('tp', 'kv'), may hold values from -1 to 1
- value_block: bfloat16 [16, 16, 128, 512], P('tp', 'kv'), may hold values from -6 to 6
- lengths: int32 [16], P('tp'), may hold values from 1 to 16384, 65536 in all
- group_gain: float32 [8192], P('kv'), may hold values from 0.1 to 1.9
- output_weight: bfloat16 [8192, 4096], P('kv', 'tp'), may hold values from -0.0625 to 0.0625
- channel_gain: float32 [4096], P('tp'), may hold values from 0.1 to 1.9
- hidden_gate: bfloat16 [4096, 11264], P('tp', 'kv'), may hold values from -0.09375 to 0.09375
- hidden_up: bfloat16 [4096, 11264], P('tp', 'kv'), may hold values from -0.09375 to 0.09375
- hidden_down: bfloat16 [11264, 4096], P('kv', 'tp'), may hold values from -0.0546875 to 0.0546875
Outputs:
- layer_out: bfloat16 [16, 4096], P('kv', 'tp')
Inputs may be any that keep to these rules, and one draw needn't show every extreme that they name: Sequence s has lengths[s] earlier positions; slots 0 to (lengths[s] mod 128) - 1 of key_block and value_block hold the turned, scaled keys and the values of its positions from 128 * floor(lengths[s] / 128) on, prior_state holds the state of the positions before them, and the other slots take no part.
All inputs are finite; a program needn't handle non-finite values. No bound on the sum of `lengths` on one device may be relied on, other than what follows from the above.
Results may differ from a plain program's by a relative error of at most 0.029.
Values may be sent and summed in bfloat16 or wider, within the bound.
A program may use at most 64 MiB of HBM per device.

v0:
```python
import jax
import jax.numpy as jnp
from jax import lax
from jax.sharding import PartitionSpec as P

D = 4096
epsilon = 1e-06


def as_sent(value):
    return jax.tree.map(lambda a: a.astype(jnp.bfloat16) if a.dtype == jnp.float32 else a, value)


def rotate(vectors, position):
    half_dim = vectors.shape[-1] // 2
    inverse = 10000.0 ** (-jnp.arange(half_dim, dtype=jnp.float32) / half_dim)
    angles = position.astype(jnp.float32)[:, None, None] * inverse
    cosine_part = jnp.cos(angles)
    sine_part = jnp.sin(angles)
    front_half = vectors[..., :half_dim]
    back_half = vectors[..., half_dim:]
    return jnp.concatenate(
        [
            front_half * cosine_part - back_half * sine_part,
            front_half * sine_part + back_half * cosine_part,
        ],
        axis=-1,
    )


def retain(
    queries,
    keys_new,
    values_new,
    gates,
    decay_rate,
    prior_state,
    key_block,
    value_block,
    lengths,
    group_gain,
):
    batch_rows = queries.shape[0]
    heads_here = decay_rate.shape[0]
    key_width = prior_state.shape[2]
    value_width = prior_state.shape[3]
    block_len = key_block.shape[2]
    rotated = rotate(
        queries.astype(jnp.float32).reshape(batch_rows, heads_here, key_width), lengths
    ).astype(jnp.bfloat16)
    fresh_keys = rotate(
        keys_new.astype(jnp.float32).reshape(batch_rows, heads_here, key_width), lengths
    ) * key_width ** (-0.5)
    fresh_values = values_new.astype(jnp.float32).reshape(batch_rows, heads_here, value_width)
    filled = lengths % block_len
    slots = jnp.arange(block_len, dtype=jnp.int32)
    distance = (filled[:, None] - slots[None, :]).astype(jnp.float32)
    live_slots = (slots[None, :] < filled[:, None])[:, None, :]
    weighting = jnp.where(
        live_slots, jnp.exp(-decay_rate[None, :, None] * distance[:, None, :]), jnp.float32(0.0)
    )
    scores = jnp.einsum("shk,shjk->shj", rotated, key_block, preferred_element_type=jnp.float32)
    block_weights = (scores * weighting).astype(jnp.bfloat16)
    block_term = jnp.einsum(
        "shj,shjv->shv", block_weights, value_block, preferred_element_type=jnp.float32
    )
    rotated_wide = rotated.astype(jnp.float32)
    own_term = jnp.sum(rotated_wide * fresh_keys, axis=-1, keepdims=True) * fresh_values
    carried = jnp.exp(-decay_rate[None, :, None] * (filled[:, None, None] + 1).astype(jnp.float32))
    state_term = carried * jnp.einsum(
        "shk,shkv->shv", rotated_wide, prior_state, precision=lax.Precision.HIGHEST
    )
    retained = own_term + block_term + state_term
    centre = jnp.mean(retained, axis=-1, keepdims=True)
    spread = jnp.mean(jnp.square(retained - centre), axis=-1, keepdims=True)
    normed = (retained - centre) * lax.rsqrt(spread + epsilon)
    gated = (
        jax.nn.silu(gates.astype(jnp.float32)).reshape(batch_rows, heads_here, value_width)
        * normed
        * group_gain.reshape(heads_here, value_width)
    )
    return gated.astype(jnp.bfloat16).reshape(batch_rows, heads_here * value_width)


def local(
    hidden_in,
    mixer_gain,
    query_weight,
    key_weight,
    value_weight,
    gate_weight,
    decay_rate,
    prior_state,
    key_block,
    value_block,
    lengths,
    group_gain,
    output_weight,
    channel_gain,
    hidden_gate,
    hidden_up,
    hidden_down,
):
    local_seqs = lengths.shape[0]
    group_count = lax.axis_size("tp")
    first_row = lax.axis_index("tp") * local_seqs
    stream = hidden_in.astype(jnp.float32)
    scaled_in = (stream * mixer_gain).astype(jnp.bfloat16)
    own_squares = jnp.sum(stream * stream, axis=1)
    own_squares = lax.psum(own_squares, "tp")
    all_rows, all_squares = (
        lax.all_gather(scaled_in, "kv", axis=0, tiled=True),
        lax.all_gather(own_squares.astype(jnp.bfloat16), "kv", axis=0, tiled=True).astype(
            own_squares.dtype
        ),
    )
    weights_in = (query_weight, key_weight, value_weight, gate_weight)
    shaped_rows = all_rows.reshape(group_count, local_seqs, all_rows.shape[1])
    half_seqs = local_seqs // 2
    pieces = []
    for portion in range(2):
        rows_part = shaped_rows[:, portion * half_seqs : (portion + 1) * half_seqs].reshape(
            group_count * half_seqs, all_rows.shape[1]
        )
        terms = tuple(
            (
                jnp.dot(rows_part, matrix, preferred_element_type=jnp.float32)
                for matrix in weights_in
            )
        )
        pieces.append(
            jax.tree.map(
                lambda part: part.astype(jnp.float32),
                lax.psum_scatter(as_sent(terms), "tp", scatter_dimension=0, tiled=True),
            )
        )
    summed = tuple(
        (
            jnp.concatenate([pieces[0][member], pieces[1][member]], axis=0)
            for member in range(len(pieces[0]))
        )
    )
    row_squares = lax.dynamic_slice_in_dim(all_squares, first_row, local_seqs, 0)
    first_scale = lax.rsqrt(row_squares / D + epsilon)[:, None]
    queries = (first_scale * summed[0]).astype(jnp.bfloat16)
    keys_new = (first_scale * summed[1]).astype(jnp.bfloat16)
    values_new = (first_scale * summed[2]).astype(jnp.bfloat16)
    gates = (first_scale * summed[3]).astype(jnp.bfloat16)
    mixed = retain(
        queries,
        keys_new,
        values_new,
        gates,
        decay_rate,
        prior_state,
        key_block,
        value_block,
        lengths,
        group_gain,
    )
    head_terms = jnp.dot(
        lax.all_gather(mixed, "tp", axis=0, tiled=True),
        output_weight,
        preferred_element_type=jnp.float32,
    )
    mixer_out = lax.psum_scatter(
        head_terms.astype(jnp.bfloat16), "kv", scatter_dimension=0, tiled=True
    ).astype(jnp.float32)
    middle = stream + mixer_out
    scaled_mid = (middle * channel_gain).astype(jnp.bfloat16)
    middle_squares = jnp.sum(middle * middle, axis=1)
    middle_squares = lax.psum(middle_squares, "tp")
    middle_rows, middle_all = (
        lax.all_gather(scaled_mid, "kv", axis=0, tiled=True),
        lax.all_gather(middle_squares.astype(jnp.bfloat16), "kv", axis=0, tiled=True).astype(
            middle_squares.dtype
        ),
    )
    channel_terms = (
        jnp.dot(middle_rows, hidden_gate, preferred_element_type=jnp.float32),
        jnp.dot(middle_rows, hidden_up, preferred_element_type=jnp.float32),
    )
    channel_summed = (
        lax.psum_scatter(
            channel_terms[0].astype(jnp.bfloat16), "tp", scatter_dimension=0, tiled=True
        ).astype(jnp.float32),
        lax.psum_scatter(
            channel_terms[1].astype(jnp.bfloat16), "tp", scatter_dimension=0, tiled=True
        ).astype(jnp.float32),
    )
    middle_row_squares = lax.dynamic_slice_in_dim(middle_all, first_row, local_seqs, 0)
    second_scale = lax.rsqrt(middle_row_squares / D + epsilon)[:, None]
    gate_part = second_scale * channel_summed[0]
    up_part = second_scale * channel_summed[1]
    activated = (jax.nn.silu(gate_part) * up_part).astype(jnp.bfloat16)
    unit_terms = jnp.dot(
        lax.all_gather(activated, "tp", axis=0, tiled=True),
        hidden_down,
        preferred_element_type=jnp.float32,
    )
    channel_out = lax.psum_scatter(
        unit_terms.astype(jnp.bfloat16), "kv", scatter_dimension=0, tiled=True
    ).astype(jnp.float32)
    return (middle + channel_out).astype(jnp.bfloat16)


def solution(mesh):
    in_specs = (
        P("kv", "tp"),
        P("tp"),
        P("tp", "kv"),
        P("tp", "kv"),
        P("tp", "kv"),
        P("tp", "kv"),
        P("kv"),
        P("tp", "kv", None, None),
        P("tp", "kv", None, None),
        P("tp", "kv", None, None),
        P("tp"),
        P("kv"),
        P("kv", "tp"),
        P("tp"),
        P("tp", "kv"),
        P("tp", "kv"),
        P("kv", "tp"),
    )
    out_specs = P("kv", "tp")
    return jax.shard_map(local, mesh=mesh, in_specs=in_specs, out_specs=out_specs, check_vma=False)
```

profile of v0, /device:TPU:0, one launch (start us, length us, event | category | flops | bytes accessed | tf_op | source)
XLA Modules:
  0.0 253.7 jit_solution(16599473605607127361)
XLA Ops:
  6.5 1.0 fusion.7
  7.5 9.7 %all-gather = bf16[4,4,512]{2,1,0:T(4,128)(2,1)S(1)} all-gather(bf16[1,4,512]{2,1,0:T(4,128)(2,1)S(1)} %get-tuple-element.28), channel_id=1, replica_groups=mesh['kv'=4,'tp'=8] {'kv'}, dimensions={0}, use_global_device_ids=true | all-gather | bytes 20480 | tf_op jit(solution)/shard_map/all_gather | solution.py:112
  17.3 2.7 %convolution_convert_fusion.2 = bf16[8,2048]{1,0:T(8,128)(2,1)} fusion(bf16[512,2048]{1,0:T(8,128)(2,1)} %param.21, bf16[8,1,512]{2,0,1:T(8,128)(2,1)S(1)} %copy.26), kind=kOutput, calls=%fused_computation.2 | convolution fusion | flops 16793600 | bytes 2138112 | tf_op jit(solution)/shard_map/dot_general | solution.py:127
  20.0 1.0 convolution_convert_fusion.3
  21.0 1.0 convolution_convert_fusion.4
  22.0 1.0 convolution_convert_fusion.5
  23.0 0.9 convolution_convert_fusion.10
  23.9 0.8 convolution_convert_fusion.11
  24.7 0.9 convolution_convert_fusion.8
  25.6 0.8 convolution_convert_fusion.9
  26.7 14.6 %psum.14 = bf16[4]{0:T(256)(128)(2,1)S(1)} all-reduce(f32[4]{0:T(128)S(1)} %get-tuple-element.27), channel_id=1, replica_groups=mesh['kv'=4,'tp'=8] {'tp'}, use_global_device_ids=true, to_apply=%region_1.0 | all-reduce | flops 4 | bytes 24 | tf_op jit(solution)/shard_map/psum | solution.py:110
  43.5 8.9 %all-reduce = bf16[16]{0:T(256)(128)(2,1)S(1)} all-reduce(bf16[16]{0:T(256)(128)(2,1)S(1)} %dynamic-update-slice), channel_id=1, replica_groups=mesh['kv'=4,'tp'=8] {'kv'}, use_global_device_ids=true, to_apply=%add | all-reduce | flops 16 | bytes 64
  54.1 29.0 %all-reduce.19.cloned.1.call-done = (bf16[8,1024]{1,0:T(8,128)(2,1)}, bf16[8,1024]{1,0:T(8,128)(2,1)}, bf16[8,2048]{1,0:T(8,128)(2,1)}, bf16[8,2048]{1,0:T(8,128...) async-done(((bf16[8,1024]{1,0:T(8,128)(2,1)}, bf16[8,1024]{1,0:T(8,128)(2,1)}, ...) | async-done | bytes 196624
  83.0 1.4 dynamic-slice_reduce_fusion.6
  84.5 1.4 dynamic-slice_reduce_fusion.4
  86.3 3.6 %fusion.19 = f32[2,4,1,512]{3,2,1,0:T(1,128)S(1)} fusion(f32[2,4,256,512]{3,2,1,0:T(8,128)} %param.24, bf16[2,4,256,1]{2,1,0,3:T(4,128)(2,1)S(1)} %fusion.30), kind=kOutput, calls=%fused_computation.53 | convolution fusion | flops 12582912 | bytes 4214784 | tf_op jit(solution)/shard_map/shk,shkv->shv/dot_general | solution.py:70
  89.9 1.5 dynamic-slice_reduce_fusion
  91.6 1.5 fusion.27
  93.4 1.5 dynamic-slice_reduce_fusion.2
  95.1 14.0 %all-gather.1 = bf16[8,2,2048]{2,1,0:T(2,128)(2,1)S(1)} all-gather(bf16[1,2,2048]{2,1,0:T(2,128)(2,1)S(1)} %reshape.210), channel_id=1, replica_groups=mesh['kv'=4,'tp'=8] {'tp'}, dimensions={0}, use_global_device_ids=true | all-gather | bytes 73728 | tf_op jit(solution)/shard_map/all_gather | solution.py:162
  109.1 2.0 convolution_convert_fusion.7
  111.0 16.0 %all-reduce.10 = bf16[16,512]{1,0:T(8,128)(2,1)S(1)} all-reduce(bf16[16,512]{1,0:T(8,128)(2,1)S(1)} %convolution_convert_fusion.7), channel_id=10, replica_groups=mesh['kv'=4,'tp'=8] {'kv'}, use_global_device_ids=true, to_apply=%region_13.14.clone | all-reduce | flops 8192 | bytes 32768
  127.2 7.2 %all-gather.2 = bf16[4,4,512]{2,1,0:T(4,128)(2,1)S(1)} all-gather(bf16[1,4,512]{2,1,0:T(4,128)(2,1)S(1)} %get-tuple-element.20), channel_id=1, replica_groups=mesh['kv'=4,'tp'=8] {'kv'}, dimensions={0}, use_global_device_ids=true | all-gather | bytes 20480 | tf_op jit(solution)/shard_map/all_gather | solution.py:174
  134.4 13.6 %psum.15 = bf16[4]{0:T(256)(128)(2,1)S(1)} all-reduce(f32[4]{0:T(128)S(1)} %get-tuple-element.19), channel_id=1, replica_groups=mesh['kv'=4,'tp'=8] {'tp'}, use_global_device_ids=true, to_apply=%region_15.16 | all-reduce | flops 4 | bytes 24 | tf_op jit(solution)/shard_map/psum | solution.py:172
  148.0 1.1 convolution_convert_fusion
  149.3 3.0 %convolution_convert_fusion.1 = bf16[16,2816]{1,0:T(8,128)(2,1)} fusion(bf16[16,512]{1,0:T(8,128)(2,1)S(1)} %reshape.213, bf16[512,2816]{1,0:T(8,128)(2,1)} %param.31), kind=kOutput, calls=%fused_computation.1 | convolution fusion | flops 46182400 | bytes 2990080 | tf_op jit(solution)/shard_map/dot_general | solution.py:180
  152.3 8.9 %all-reduce.1 = bf16[16]{0:T(256)(128)(2,1)S(1)} all-reduce(bf16[16]{0:T(256)(128)(2,1)S(1)} %dynamic-update-slice.1), channel_id=1, replica_groups=mesh['kv'=4,'tp'=8] {'kv'}, use_global_device_ids=true, to_apply=%add.1 | all-reduce | flops 16 | bytes 64
  161.3 51.1 %all-reduce.21.cloned.1.call-done = (bf16[16,2816]{1,0:T(8,128)(2,1)}, bf16[16,2816]{1,0:T(8,128)(2,1)}) async-done(((bf16[16,2816]{1,0:T(8,128)(2,1)}, bf16[16,2816]{1,0:T(8,128)(2,1)}), (bf16[16,2816]{1,0:T(8,128)(2,1)}, bf16[16,2816]{1,0:T(8,128)(2,1)})) %all-reduce.21.cloned.1.call-update) | async-done | bytes 180240
  212.4 0.9 fusion.6
  213.4 14.6 %all-gather.3 = bf16[8,2,2816]{2,1,0:T(2,128)(2,1)S(1)} all-gather(bf16[1,2,2816]{2,1,0:T(2,128)(2,1)S(1)} %fusion.6), channel_id=1, replica_groups=mesh['kv'=4,'tp'=8] {'tp'}, dimensions={0}, use_global_device_ids=true | all-gather | bytes 101376 | tf_op jit(solution)/shard_map/all_gather | solution.py:197
  227.9 2.3 convolution_convert_fusion.6
  230.2 16.0 %all-reduce.13 = bf16[16,512]{1,0:T(8,128)(2,1)S(1)} all-reduce(bf16[16,512]{1,0:T(8,128)(2,1)S(1)} %convolution_convert_fusion.6), channel_id=13, replica_groups=mesh['kv'=4,'tp'=8] {'kv'}, use_global_device_ids=true, to_apply=%region_18.19.clone | all-reduce | flops 8192 | bytes 32768
  (77 shorter events, 4.3 us)
Async XLA Ops:
  6.5 141.5 %copy-start = (bf16[512,2816]{1,0:T(8,128)(2,1)S(1)}, bf16[512,2816]{1,0:T(8,128)(2,1)}, u32[]{:S(2)}) copy-start(bf16[512,2816]{1,0:T(8,128)(2,1)} %param.32) | copy-start | bytes 8650756
  6.5 76.5 %all-reduce.19.cloned.1.call-start = ((), (), s32[]{:S(2)}) async-start(), calls=%async_computation | async-start | bytes 393216
  17.2 2.8 %copy-start.1 = (bf16[512,2048]{1,0:T(8,128)(2,1)S(1)}, bf16[512,2048]{1,0:T(8,128)(2,1)}, u32[]{:S(2)}) copy-start(bf16[512,2048]{1,0:T(8,128)(2,1)} %param.21) | copy-start | bytes 6291460
  17.3 3.7 %copy-start.2 = (bf16[512,2048]{1,0:T(8,128)(2,1)S(1)}, bf16[512,2048]{1,0:T(8,128)(2,1)}, u32[]{:S(2)}) copy-start(bf16[512,2048]{1,0:T(8,128)(2,1)} %param.22) | copy-start | bytes 6291460
  21.0 2.0 copy-start.3
  22.0 2.7 %copy-start.4 = (bf16[512,1024]{1,0:T(8,128)(2,1)S(1)}, bf16[512,1024]{1,0:T(8,128)(2,1)}, u32[]{:S(2)}) copy-start(bf16[512,1024]{1,0:T(8,128)(2,1)} %param.20) | copy-start | bytes 3145732
  23.0 3.5 %copy-start.10 = (s32[2]{0:T(128)S(1)}, s32[2]{0:T(128)}, u32[]{:S(2)}) copy-start(s32[2]{0:T(128)} %param.27) | copy-start | bytes 28
  23.0 18.3 %copy-start.12 = (u32[32]{0:T(128)S(1)}, u32[32]{0:T(128)}, u32[]{:S(2)}) copy-start(u32[32]{0:T(128)} %constant.69) | copy-start | bytes 388
  23.0 18.9 %copy-start.9 = (u32[32]{0:T(128)S(1)}, u32[32]{0:T(128)}, u32[]{:S(2)}) copy-start(u32[32]{0:T(128)} %constant.57) | copy-start | bytes 388
  23.0 29.5 %copy-start.11 = (f32[4]{0:T(128)S(1)}, f32[4]{0:T(128)}, u32[]{:S(2)}) copy-start(f32[4]{0:T(128)} %param.23) | copy-start | bytes 52
  23.0 29.5 %copy-start.7 = (f32[2048]{0:T(1024)S(1)}, f32[2048]{0:T(1024)}, u32[]{:S(2)}) copy-start(f32[2048]{0:T(1024)} %param.28) | copy-start | bytes 24580
  23.9 62.2 %copy-start.5 = (bf16[2,4,128,256]{3,2,1,0:T(8,128)(2,1)S(1)}, bf16[2,4,128,256]{3,2,1,0:T(8,128)(2,1)}, u32[]{:S(2)}) copy-start(bf16[2,4,128,256]{3,2,1,0:T(8,128)(2,1)} %param.25) | copy-start | bytes 1572868
  26.4 186.0 %all-reduce.21.cloned.1.call-start = ((), (), s32[]{:S(2)}) async-start(), calls=%async_computation.1 | async-start | bytes 360448
  89.9 37.1 %copy-start.6 = (bf16[4,512]{1,0:T(4,128)(2,1)S(1)}, bf16[4,512]{1,0:T(4,128)(2,1)}, u32[]{:S(2)}) copy-start(bf16[4,512]{1,0:T(4,128)(2,1)} %param.17) | copy-start | bytes 12292
  89.9 37.1 %copy-start.8 = (f32[512]{0:T(512)S(1)}, f32[512]{0:T(512)}, u32[]{:S(2)}) copy-start(f32[512]{0:T(512)} %param.30) | copy-start | bytes 6148
Sparse Core Ops, SparseCore 0:
  26.6 56.4 all-reduce.18
  161.3 51.0 all-reduce.20
where the time goes:
time: 255 us; the launch traced here: 254 us
  blocking collectives  123 us (48%)
  waiting for transfers between devices  80.2 us (31%)
  matrix products  22.8 us (9%)
  between operations  15.6 us (6%)
  local copies, waits for them, and re-layouts  7.82 us (3%)
  other arithmetic  3.84 us (2%)
    unnamed x4, waiting for transfers between devices  80.2 us
    unnamed x4, blocking collectives  49.8 us
    psum x1, blocking collectives, local(): own_squares = lax.psum(own_squares, 'tp')  14.6 us
    all_gather x1, blocking collectives, local(): lax.all_gather(activated, 'tp', axis=0, tiled=True)  14.6 us
    all_gather x1, blocking collectives, local(): lax.all_gather(mixed, 'tp', axis=0, tiled=True)  14 us
    psum x1, blocking collectives, local(): middle_squares = lax.psum(middle_squares, 'tp')  13.6 us
    all_gather x1, blocking collectives, local(): lax.all_gather(scaled_in, 'kv', axis=0, tiled=True)  9.66 us
    dot_general x8, matrix products, local(): jnp.dot(rows_part, matrix, preferred_element_type=jnp.float32)  9.1 us
  transfers between devices with their start and end apart: 2, of which 2 were waited for; matrix products, arithmetic and copies ran while one was open for 1% of the time, Pallas kernels for 0%

commit v1 on v0

--- a/solution.py
+++ b/solution.py
@@ -169,7 +169,11 @@
     middle = stream + mixer_out
     scaled_mid = (middle * channel_gain).astype(jnp.bfloat16)
     middle_squares = jnp.sum(middle * middle, axis=1)
-    middle_squares = lax.psum(middle_squares, "tp")
+    middle_squares = middle_squares
+    for hop in (1, 2, 4):
+        middle_squares = middle_squares + lax.ppermute(
+            middle_squares, "tp", [(dev, dev ^ hop) for dev in range(8)]
+        )
     middle_rows, middle_all = (
         lax.all_gather(scaled_mid, "kv", axis=0, tiled=True),
         lax.all_gather(middle_squares.astype(jnp.bfloat16), "kv", axis=0, tiled=True).astype(

time: 255 us -> 240 us (0.941)
  blocking collectives: 123 us -> 110 us
    psum x1 -> x0, blocking collectives: 13.6 us -> none  [local(): middle_squares = lax.psum(middle_squares, 'tp')]
    unnamed x4, waiting for transfers between devices: 80.2 us -> 71.9 us
    ppermute x0 -> x3, waiting for transfers between devices: none -> 7.46 us  [local(): lax.ppermute(middle_squares, 'tp', [(dev, dev ^ hop) for dev in range(8)])]
    unnamed x42 -> x44, local copies, waits for them, and re-layouts: 7.67 us -> 8.45 us
  transfers between devices with their start and end apart: 2 -> 5, of which waited for: 2 -> 4; matrix products, arithmetic and copies ran while one was open for 1% -> 2% of each run, Pallas kernels for 0% -> 0%
where the time goes in v1:
time: 240 us; the launch traced here: 239 us
  blocking collectives  110 us (46%)
  waiting for transfers between devices  79.4 us (33%)
  matrix products  20.9 us (9%)
  between operations  15.6 us (6%)
  local copies, waits for them, and re-layouts  8.6 us (4%)
  other arithmetic  3.85 us (2%)
    unnamed x4, waiting for transfers between devices  71.9 us
    unnamed x4, blocking collectives  49.8 us
    psum x1, blocking collectives, local(): own_squares = lax.psum(own_squares, 'tp')  14.6 us
    all_gather x1, blocking collectives, local(): lax.all_gather(activated, 'tp', axis=0, tiled=True)  14.6 us
    all_gather x1, blocking collectives, local(): lax.all_gather(mixed, 'tp', axis=0, tiled=True)  14 us
    all_gather x1, blocking collectives, local(): lax.all_gather(scaled_in, 'kv', axis=0, tiled=True)  9.66 us
    dot_general x8, matrix products, local(): jnp.dot(rows_part, matrix, preferred_element_type=jnp.float32)  9.1 us
    unnamed x44, local copies, waits for them, and re-layouts  8.45 us
  transfers between devices with their start and end apart: 5, of which 4 were waited for; matrix products, arithmetic and copies ran while one was open for 2% of the time, Pallas kernels for 0%

profile of v1, /device:TPU:0, one launch (start us, length us, event | category | flops | bytes accessed | tf_op | source)
XLA Modules:
  0.0 239.0 jit_solution(1790705692135191120)
XLA Ops:
  6.5 1.0 fusion.7
  7.5 9.7 %all-gather = bf16[4,4,512]{2,1,0:T(4,128)(2,1)S(1)} all-gather(bf16[1,4,512]{2,1,0:T(4,128)(2,1)S(1)} %get-tuple-element.28), channel_id=1, replica_groups=mesh['kv'=4,'tp'=8] {'kv'}, dimensions={0}, use_global_device_ids=true | all-gather | bytes 20480 | tf_op jit(solution)/shard_map/all_gather | solution.py:112
  17.3 2.7 %convolution_convert_fusion.2 = bf16[8,2048]{1,0:T(8,128)(2,1)} fusion(bf16[512,2048]{1,0:T(8,128)(2,1)} %param.21, bf16[8,1,512]{2,0,1:T(8,128)(2,1)S(1)} %copy.26), kind=kOutput, calls=%fused_computation.2 | convolution fusion | flops 16793600 | bytes 2138112 | tf_op jit(solution)/shard_map/dot_general | solution.py:127
  20.0 1.0 convolution_convert_fusion.3
  21.0 1.0 convolution_convert_fusion.4
  22.0 1.0 convolution_convert_fusion.5
  23.0 0.9 convolution_convert_fusion.10
  23.9 0.8 convolution_convert_fusion.11
  24.7 0.9 convolution_convert_fusion.8
  26.7 14.6 %psum.7 = bf16[4]{0:T(256)(128)(2,1)S(1)} all-reduce(f32[4]{0:T(128)S(1)} %get-tuple-element.27), channel_id=1, replica_groups=mesh['kv'=4,'tp'=8] {'tp'}, use_global_device_ids=true, to_apply=%region_1.0 | all-reduce | flops 4 | bytes 24 | tf_op jit(solution)/shard_map/psum | solution.py:110
  43.5 8.9 %all-reduce = bf16[16]{0:T(256)(128)(2,1)S(1)} all-reduce(bf16[16]{0:T(256)(128)(2,1)S(1)} %dynamic-update-slice), channel_id=1, replica_groups=mesh['kv'=4,'tp'=8] {'kv'}, use_global_device_ids=true, to_apply=%add | all-reduce | flops 16 | bytes 64
  54.1 29.0 %all-reduce.19.cloned.1.call-done = (bf16[8,1024]{1,0:T(8,128)(2,1)}, bf16[8,1024]{1,0:T(8,128)(2,1)}, bf16[8,2048]{1,0:T(8,128)(2,1)}, bf16[8,2048]{1,0:T(8,128...) async-done(((bf16[8,1024]{1,0:T(8,128)(2,1)}, bf16[8,1024]{1,0:T(8,128)(2,1)}, ...) | async-done | bytes 196624
  83.0 1.4 dynamic-slice_reduce_fusion.6
  84.5 1.4 dynamic-slice_reduce_fusion.4
  86.3 3.6 %fusion.19 = f32[2,4,1,512]{3,2,1,0:T(1,128)S(1)} fusion(f32[2,4,256,512]{3,2,1,0:T(8,128)} %param.24, bf16[2,4,256,1]{2,1,0,3:T(4,128)(2,1)S(1)} %fusion.30), kind=kOutput, calls=%fused_computation.53 | convolution fusion | flops 12582912 | bytes 4214784 | tf_op jit(solution)/shard_map/shk,shkv->shv/dot_general | solution.py:70
  89.9 1.5 dynamic-slice_reduce_fusion
  91.6 1.5 fusion.27
  93.4 1.5 dynamic-slice_reduce_fusion.2
  95.1 14.0 %all-gather.1 = bf16[8,2,2048]{2,1,0:T(2,128)(2,1)S(1)} all-gather(bf16[1,2,2048]{2,1,0:T(2,128)(2,1)S(1)} %reshape.210), channel_id=1, replica_groups=mesh['kv'=4,'tp'=8] {'tp'}, dimensions={0}, use_global_device_ids=true | all-gather | bytes 73728 | tf_op jit(solution)/shard_map/all_gather | solution.py:162
  109.1 2.0 convolution_convert_fusion.7
  111.0 16.0 %all-reduce.10 = bf16[16,512]{1,0:T(8,128)(2,1)S(1)} all-reduce(bf16[16,512]{1,0:T(8,128)(2,1)S(1)} %convolution_convert_fusion.7), channel_id=10, replica_groups=mesh['kv'=4,'tp'=8] {'kv'}, use_global_device_ids=true, to_apply=%region_13.14.clone | all-reduce | flops 8192 | bytes 32768
  127.2 7.2 %all-gather.2 = bf16[4,4,512]{2,1,0:T(4,128)(2,1)S(1)} all-gather(bf16[1,4,512]{2,1,0:T(4,128)(2,1)S(1)} %get-tuple-element.20), channel_id=1, replica_groups=mesh['kv'=4,'tp'=8] {'kv'}, dimensions={0}, use_global_device_ids=true | all-gather | bytes 20480 | tf_op jit(solution)/shard_map/all_gather | solution.py:178
  134.5 1.1 convolution_convert_fusion
  136.3 1.1 convolution_convert_fusion.1
  137.5 3.6 %collective-permute-done.1 = f32[4]{0:T(128)S(1)} collective-permute-done((f32[4]{0:T(128)S(1)}, f32[4]{0:T(128)S(1)}, u32[]{:S(2)}, u32[]{:S(2)}) %collective-permute-start.1) | collective-permute-done | bytes 48 | tf_op jit(solution)/shard_map/ppermute | solution.py:174
  141.6 3.9 %collective-permute-done.2 = f32[4]{0:T(128)S(1)} collective-permute-done((f32[4]{0:T(128)S(1)}, f32[4]{0:T(128)S(1)}, u32[]{:S(2)}, u32[]{:S(2)}) %collective-permute-start.2) | collective-permute-done | bytes 48 | tf_op jit(solution)/shard_map/ppermute | solution.py:174
  145.8 8.9 %all-reduce.1 = bf16[16]{0:T(256)(128)(2,1)S(1)} all-reduce(bf16[16]{0:T(256)(128)(2,1)S(1)} %dynamic-update-slice.1), channel_id=1, replica_groups=mesh['kv'=4,'tp'=8] {'kv'}, use_global_device_ids=true, to_apply=%add.1 | all-reduce | flops 16 | bytes 64
  154.8 42.9 %all-reduce.21.cloned.1.call-done = (bf16[16,2816]{1,0:T(8,128)(2,1)}, bf16[16,2816]{1,0:T(8,128)(2,1)}) async-done(((bf16[16,2816]{1,0:T(8,128)(2,1)}, bf16[16,2816]{1,0:T(8,128)(2,1)}), (bf16[16,2816]{1,0:T(8,128)(2,1)}, bf16[16,2816]{1,0:T(8,128)(2,1)})) %all-reduce.21.cloned.1.call-update) | async-done | bytes 180240
  197.7 0.9 fusion.6
  198.6 14.6 %all-gather.3 = bf16[8,2,2816]{2,1,0:T(2,128)(2,1)S(1)} all-gather(bf16[1,2,2816]{2,1,0:T(2,128)(2,1)S(1)} %fusion.6), channel_id=1, replica_groups=mesh['kv'=4,'tp'=8] {'tp'}, dimensions={0}, use_global_device_ids=true | all-gather | bytes 101376 | tf_op jit(solution)/shard_map/all_gather | solution.py:201
  213.2 2.3 convolution_convert_fusion.6
  215.5 16.0 %all-reduce.13 = bf16[16,512]{1,0:T(8,128)(2,1)S(1)} all-reduce(bf16[16,512]{1,0:T(8,128)(2,1)S(1)} %convolution_convert_fusion.6), channel_id=13, replica_groups=mesh['kv'=4,'tp'=8] {'kv'}, use_global_device_ids=true, to_apply=%region_17.18.clone | all-reduce | flops 8192 | bytes 32768
  (87 shorter events, 6.5 us)
Async XLA Ops:
  6.5 128.0 %copy-start = (bf16[512,2816]{1,0:T(8,128)(2,1)S(1)}, bf16[512,2816]{1,0:T(8,128)(2,1)}, u32[]{:S(2)}) copy-start(bf16[512,2816]{1,0:T(8,128)(2,1)} %param.32) | copy-start | bytes 8650756
  6.5 76.5 %all-reduce.19.cloned.1.call-start = ((), (), s32[]{:S(2)}) async-start(), calls=%async_computation | async-start | bytes 393216
  17.2 2.8 %copy-start.1 = (bf16[512,2048]{1,0:T(8,128)(2,1)S(1)}, bf16[512,2048]{1,0:T(8,128)(2,1)}, u32[]{:S(2)}) copy-start(bf16[512,2048]{1,0:T(8,128)(2,1)} %param.21) | copy-start | bytes 6291460
  17.3 3.7 %copy-start.2 = (bf16[512,2048]{1,0:T(8,128)(2,1)S(1)}, bf16[512,2048]{1,0:T(8,128)(2,1)}, u32[]{:S(2)}) copy-start(bf16[512,2048]{1,0:T(8,128)(2,1)} %param.22) | copy-start | bytes 6291460
  21.0 2.0 copy-start.3
  22.0 2.7 %copy-start.4 = (bf16[512,1024]{1,0:T(8,128)(2,1)S(1)}, bf16[512,1024]{1,0:T(8,128)(2,1)}, u32[]{:S(2)}) copy-start(bf16[512,1024]{1,0:T(8,128)(2,1)} %param.20) | copy-start | bytes 3145732
  23.0 3.5 %copy-start.11 = (s32[2]{0:T(128)S(1)}, s32[2]{0:T(128)}, u32[]{:S(2)}) copy-start(s32[2]{0:T(128)} %param.27) | copy-start | bytes 28
  23.0 18.3 %copy-start.13 = (u32[32]{0:T(128)S(1)}, u32[32]{0:T(128)}, u32[]{:S(2)}) copy-start(u32[32]{0:T(128)} %constant.69) | copy-start | bytes 388
  23.0 18.9 %copy-start.10 = (u32[32]{0:T(128)S(1)}, u32[32]{0:T(128)}, u32[]{:S(2)}) copy-start(u32[32]{0:T(128)} %constant.57) | copy-start | bytes 388
  23.0 29.5 %copy-start.12 = (f32[4]{0:T(128)S(1)}, f32[4]{0:T(128)}, u32[]{:S(2)}) copy-start(f32[4]{0:T(128)} %param.23) | copy-start | bytes 52
  23.0 29.5 %copy-start.8 = (f32[2048]{0:T(1024)S(1)}, f32[2048]{0:T(1024)}, u32[]{:S(2)}) copy-start(f32[2048]{0:T(1024)} %param.28) | copy-start | bytes 24580
  23.9 62.2 %copy-start.6 = (bf16[2,4,128,256]{3,2,1,0:T(8,128)(2,1)S(1)}, bf16[2,4,128,256]{3,2,1,0:T(8,128)(2,1)}, u32[]{:S(2)}) copy-start(bf16[2,4,128,256]{3,2,1,0:T(8,128)(2,1)} %param.25) | copy-start | bytes 1572868
  26.4 171.3 %all-reduce.21.cloned.1.call-start = ((), (), s32[]{:S(2)}) async-start(), calls=%async_computation.1 | async-start | bytes 360448
  89.9 37.1 %copy-start.7 = (bf16[4,512]{1,0:T(4,128)(2,1)S(1)}, bf16[4,512]{1,0:T(4,128)(2,1)}, u32[]{:S(2)}) copy-start(bf16[4,512]{1,0:T(4,128)(2,1)} %param.17) | copy-start | bytes 12292
  89.9 37.1 %copy-start.9 = (f32[512]{0:T(512)S(1)}, f32[512]{0:T(512)}, u32[]{:S(2)}) copy-start(f32[512]{0:T(512)} %param.30) | copy-start | bytes 6148
  127.2 10.3 %collective-permute-start = (f32[4]{0:T(128)S(1)}, f32[4]{0:T(128)S(1)}, u32[]{:S(2)}, u32[]{:S(2)}) collective-permute-start(f32[4]{0:T(128)S(1)} %get-tuple-element.19), channel_id=1, source_target_pairs={{0,1},{1,0},{2,3},{3,2},{4,5},{5,4},{6,7},{7,6},{8,9},{9,8},{10,11... | collective-permute-start | bytes 56 | tf_op jit(solution)/shard_map/ppermute | solution.py:174
  134.5 1.9 copy-start.5
  137.5 3.6 %collective-permute-start.1 = (f32[4]{0:T(128)S(1)}, f32[4]{0:T(128)S(1)}, u32[]{:S(2)}, u32[]{:S(2)}) collective-permute-start(f32[4]{0:T(128)S(1)} %add.101), channel_id=1, source_target_pairs={{0,2},{1,3},{2,0},{3,1},{4,6},{5,7},{6,4},{7,5},{8,10},{9,11},{10,... | collective-permute-start | bytes 56 | tf_op jit(solution)/shard_map/ppermute | solution.py:174
  141.1 4.5 %collective-permute-start.2 = (f32[4]{0:T(128)S(1)}, f32[4]{0:T(128)S(1)}, u32[]{:S(2)}, u32[]{:S(2)}) collective-permute-start(f32[4]{0:T(128)S(1)} %add.102), channel_id=1, source_target_pairs={{0,4},{1,5},{2,6},{3,7},{4,0},{5,1},{6,2},{7,3},{8,12},{9,13},{10,... | collective-permute-start | bytes 56 | tf_op jit(solution)/shard_map/ppermute | solution.py:174
Sparse Core Ops, SparseCore 0:
  26.6 56.4 all-reduce.18
  145.9 51.7 all-reduce.20
